TPU v7x, 32 devices: a whole 2x2x4 slice. The times are simulated.
32 devices in a mesh: sp: 8 (over z, y), tp: 4 (over x, core).
Axes of the slice: x: 2, y: 2, z: 4, core: 2. Of those that a mesh axis runs over, the one named last changes fastest.
Arguments:
- tokens: bfloat16 [4096, 2048], P(('sp', 'tp')), may hold values from -6 to 6
- norm_gain: bfloat16 [2048], replicated, may hold values from 0.099609375 to 1.8984375
- proj_x: bfloat16 [2048, 2048], P('sp', 'tp'), may hold values from -0.125 to 0.125
- gate_projection: bfloat16 [2048, 2048], P('sp', 'tp'), may hold values from -0.125 to 0.125
- conv_taps: bfloat16 [4, 2048], P(None, 'tp'), may hold values from -3 to 3
- gate_recur: bfloat16 [8, 256, 256], P('tp'), may hold values from -0.375 to 0.375
- gate_input: bfloat16 [8, 256, 256], P('tp'), may hold values from -0.375 to 0.375
- decay_param: float32 [2048], P('tp'), may hold values from 4 to 25
- decay_shift: float32 [8, 4096], P('tp', 'sp'), may hold values from -1.3 to 0, as said below
- proj_out: bfloat16 [2048, 2048], P('tp', 'sp'), may hold values from -0.125 to 0.125
Outputs:
- mixed_out: bfloat16 [4096, 2048], P(('sp', 'tp'))
Inputs may be any that keep to these rules, and one draw needn't show every extreme that they name: `decay_shift`: added log-decays, never positive.
All inputs are finite; a program needn't handle non-finite values.
Results may differ from a plain program's by a relative error of at most 0.015.
Values may be sent and summed in bfloat16 or wider, within the bound.
A program may use at most 128 MiB of HBM per device.

v0:
```python
import jax
import jax.numpy as jnp
from jax import lax
from jax.sharding import PartitionSpec as P

HEAD = 256
CONV = 4


def shifted(block, axis, distance):
    devices = range(lax.axis_size(axis))
    route = [(i - distance, i) for i in devices if i - distance in devices]
    return lax.ppermute(block, axis, route)


def carried_in(array, axis, combine, identity):
    size, index = (lax.axis_size(axis), lax.axis_index(axis))
    everything = jax.tree.map(lambda part: lax.all_gather(part, axis), array)
    start = jax.tree.map(
        lambda part, zero: jnp.broadcast_to(jnp.asarray(zero, part.dtype), part.shape),
        array,
        identity,
    )

    def turn(k, before):
        reached = k < index
        new = combine(before, jax.tree.map(lambda part: part[k], everything))
        return jax.tree.map(lambda a, b: jnp.where(reached, a, b), new, before)

    return lax.fori_loop(0, size, turn, start)


def rms_norm(values, norm_gain):
    floats = values.astype(jnp.float32)
    scaled = floats * lax.rsqrt(jnp.mean(floats * floats, axis=-1, keepdims=True) + 1e-06)
    return (scaled * norm_gain.astype(jnp.float32)).astype(jnp.bfloat16)


def combine_pair(earlier, later):
    return (earlier[0] * later[0], later[0] * earlier[1] + later[1])


def on_device(
    tokens,
    norm_gain,
    proj_x,
    gate_projection,
    conv_taps,
    gate_recur,
    gate_input,
    decay_param,
    decay_shift,
    proj_out,
):
    normed = rms_norm(tokens, norm_gain)
    full_x, full_gate = (
        lax.all_gather(proj_x, "sp", axis=0, tiled=True),
        lax.all_gather(gate_projection, "sp", axis=0, tiled=True),
    )
    local_width = proj_x.shape[1]
    piece = lax.all_gather(normed, "tp", axis=0, tiled=True)
    branch_piece = jnp.dot(piece, full_x, preferred_element_type=jnp.float32).astype(jnp.bfloat16)
    gating_piece = jnp.dot(piece, full_gate, preferred_element_type=jnp.float32).astype(
        jnp.bfloat16
    )
    joined = jnp.concatenate([branch_piece, gating_piece], axis=1)
    branch = joined[:, :local_width]
    gating = joined[:, local_width:]
    row_count = branch.shape[0]
    tail_rows = shifted(branch[row_count - CONV + 1 :], "sp", 1)
    extended = jnp.concatenate([tail_rows, branch], axis=0)
    conv_sum = jnp.zeros((row_count, local_width), jnp.float32)
    for tap_index in range(CONV):
        conv_sum = conv_sum + extended[tap_index : tap_index + row_count].astype(
            jnp.float32
        ) * conv_taps[tap_index].astype(jnp.float32)
    conved = conv_sum.astype(jnp.bfloat16)
    head_count = gate_recur.shape[0]
    grouped = conved.reshape(row_count, head_count, HEAD)
    recur = jax.nn.sigmoid(
        jnp.einsum("thi,hij->thj", grouped, gate_recur, preferred_element_type=jnp.float32)
    )
    inlet = jax.nn.sigmoid(
        jnp.einsum("thi,hij->thj", grouped, gate_input, preferred_element_type=jnp.float32)
    )
    decay_rate = jax.nn.softplus(-decay_param).reshape(head_count, HEAD)
    log_decay = (-8.0 * recur * decay_rate[None] + jnp.transpose(decay_shift)[:, :, None]).reshape(
        row_count, local_width
    )
    decay = jnp.exp(log_decay)
    drive = (
        jnp.sqrt(-jnp.expm1(2.0 * log_decay))
        * inlet.reshape(row_count, local_width)
        * conved.astype(jnp.float32)
    )
    identity = (jnp.ones((local_width,), jnp.float32), jnp.zeros((local_width,), jnp.float32))
    cumulative, local_state = lax.associative_scan(combine_pair, (decay, drive), axis=0)
    carried = carried_in(
        (cumulative[row_count - 1], local_state[row_count - 1]), "sp", combine_pair, identity
    )
    states = local_state + cumulative * carried[1][None, :]
    mixed = (states * jax.nn.gelu(gating.astype(jnp.float32))).astype(jnp.bfloat16)
    out_cols = lax.all_gather(proj_out, "sp", axis=1, tiled=True)
    return lax.psum_scatter(
        jnp.dot(mixed, out_cols, preferred_element_type=jnp.float32).astype(jnp.bfloat16),
        "tp",
        scatter_dimension=0,
        tiled=True,
    )


def solution(mesh):
    in_specs = (
        P(("sp", "tp"), None),
        P(),
        P("sp", "tp"),
        P("sp", "tp"),
        P(None, "tp"),
        P("tp", None, None),
        P("tp", None, None),
        P("tp"),
        P("tp", "sp"),
        P("tp", "sp"),
    )
    out_specs = P(("sp", "tp"), None)
    return jax.shard_map(
        on_device, mesh=mesh, in_specs=in_specs, out_specs=out_specs, check_vma=False
    )
```

profile of v0, /device:TPU:0, one launch (start us, length us, event | category | flops | bytes accessed | tf_op | source)
XLA Modules:
  0.0 287.4 jit_solution(4033228351637639462)
XLA Ops:
  6.5 1.3 fusion.11
  8.5 2.0 fusion.13
  12.7 23.3 %all-gather.7.cloned.1.call-done = bf16[512,2048]{1,0:T(8,128)(2,1)} async-done(((bf16[128,2048]{1,0:T(8,128)(2,1)}), bf16[512,2048]{1,0:T(8,128)(2,1)}) %all-gather.7.cloned.1.call-update) | async-done | bytes 2097168 | tf_op jit(solution)/shard_map/all_gather | solution.py:61
  36.0 51.2 %all-gather.9.cloned.1.call-done = bf16[2048,512]{1,0:T(8,128)(2,1)} async-done(((bf16[256,512]{1,0:T(8,128)(2,1)}), bf16[2048,512]{1,0:T(8,128)(2,1)}) %all-gather.9.cloned.1.call-update) | async-done | bytes 2097168 | tf_op jit(solution)/shard_map/all_gather | solution.py:57
  87.3 3.5 %convolution_convert_fusion.2 = bf16[512,512]{1,0:T(8,128)(2,1)S(1)} fusion(bf16[512,2048]{1,0:T(8,128)(2,1)} %all-gather.7.cloned.1.call-done, bf16[2048,512]{1,0:T(8,128)(2,1)} %all-gather.9.cloned.1.call-done), kind=kOutput, calls=%fused_computation.24 | convolution fusion | flops 1074003968 | bytes 4718592 | tf_op jit(solution)/shard_map/dot_general | solution.py:62
  90.7 2.5 collective-permute-start
  93.3 1.2 collective-permute-done
  96.2 1.9 fusion.4
  98.1 1.6 copy.31
  100.9 2.3 slice.367
  103.2 2.1 slice.305
  105.3 2.1 slice.304
  107.5 19.5 %slice.303 = f32[256,512]{0,1:T(8,128)S(1)} slice(f32[512,512]{0,1:T(8,128)S(1)} %bitcast.49), slice={[1:512:2], [0:512:1]} | slice | bytes 1048576 | tf_op jit(solution)/shard_map/slice | solution.py:97
  127.0 19.4 %slice.302 = f32[255,512]{0,1:T(8,128)S(1)} slice(f32[512,512]{0,1:T(8,128)S(1)} %bitcast.50), slice={[2:512:2], [0:512:1]} | slice | bytes 1044480 | tf_op jit(solution)/shard_map/slice | solution.py:97
  146.4 19.5 %slice.307 = f32[256,512]{0,1:T(8,128)S(1)} slice(f32[512,512]{0,1:T(8,128)S(1)} %bitcast.51), slice={[0:511:2], [0:512:1]} | slice | bytes 1048576 | tf_op jit(solution)/shard_map/slice | solution.py:97
  167.3 1.3 multiply_add_fusion
  177.9 2.9 pad.144
  180.8 2.7 pad.126
  183.6 2.7 pad.127
  187.0 27.3 %all-gather.1 = f32[8,1,512]{2,1,0:T(1,128)S(1)} all-gather(f32[1,1,512]{2,1,0:T(1,128)S(1)} %add_bitcast_fusion), channel_id=1, replica_groups=mesh['sp'=8,'tp'=4] {'sp'}, dimensions={0}, use_global_device_ids=true | all-gather | bytes 18432 | tf_op jit(solution)/shard_map/all_gather | solution.py:18
  214.3 2.8 pad.145
  217.8 26.1 %all-gather = f32[8,1,512]{2,1,0:T(1,128)S(1)} all-gather(f32[1,1,512]{2,1,0:T(1,128)S(1)} %add_bitcast_fusion.1), channel_id=1, replica_groups=mesh['sp'=8,'tp'=4] {'sp'}, dimensions={0}, use_global_device_ids=true | all-gather | bytes 18432 | tf_op jit(solution)/shard_map/all_gather | solution.py:18
  244.4 7.9 %convolution_convert_fusion = bf16[512,2048]{1,0:T(8,128)(2,1)} fusion(bf16[512,2048]{1,0:T(8,128)(2,1)} %all-gather.13.cloned.1.call-done, bf16[512,2048]{1,0:T(8,128)(2,1)} %all-gather.7.cloned.1.call-done, bf16[2048,512]{1,0:T(8,128)(2,1)} %all-gather.11.cloned.1.call-done, f32[512,512]{1,0:T(8,128)S(1)} %copy-done.8, f32[512,512]{1,0:T(8,128)} %pad.145, ...), kind=kOutput, calls=%fused_computation.3 | convolution fusion | flops 2152726528 | bytes 12584960 | tf_op jit(solution)/shard_map/dot_general | solution.py:105
  252.3 28.5 %reduce-scatter.2.cloned.1.call-done = bf16[128,2048]{1,0:T(8,128)(2,1)} async-done(((bf16[512,2048]{1,0:T(8,128)(2,1)}), bf16[128,2048]{1,0:T(8,128)(2,1)}) %reduce-scatter.2.cloned.1.call-update) | async-done | bytes 524304 | tf_op jit(solution)/shard_map/reduce_scatter | solution.py:104
  (202 shorter events, 18.0 us)
Async XLA Ops:
  6.5 88.5 %copy-start = (bf16[2,256,256]{2,1,0:T(8,128)(2,1)S(1)}, bf16[2,256,256]{2,1,0:T(8,128)(2,1)}, u32[]{:S(2)}) copy-start(bf16[2,256,256]{2,1,0:T(8,128)(2,1)} %param.17) | copy-start | bytes 786436
  6.5 6.1 %copy-start.9 = (bf16[4,512]{1,0:T(4,128)(2,1)S(1)}, bf16[4,512]{1,0:T(4,128)(2,1)}, u32[]{:S(2)}) copy-start(bf16[4,512]{1,0:T(4,128)(2,1)} %param.16) | copy-start | bytes 12292
  6.5 29.5 %all-gather.7.cloned.1.call-start = ((), (), s32[]{:S(2)}) async-start(), calls=%async_computation.1 | async-start | bytes 2621440 | tf_op jit(solution)/shard_map/all_gather | solution.py:61
  10.6 76.7 %all-gather.9.cloned.1.call-start = ((), (), s32[]{:S(2)}) async-start(), calls=%async_computation.2 | async-start | bytes 2359296 | tf_op jit(solution)/shard_map/all_gather | solution.py:57
  11.3 233.0 %all-gather.11.cloned.1.call-start = ((), (), s32[]{:S(2)}) async-start(), calls=%async_computation.3 | async-start | bytes 2359296 | tf_op jit(solution)/shard_map/all_gather | solution.py:58
  12.1 232.3 %all-gather.13.cloned.1.call-start = ((), (), s32[]{:S(2)}) async-start(), calls=%async_computation.4 | async-start | bytes 2359296 | tf_op jit(solution)/shard_map/all_gather | solution.py:103
  12.6 268.2 %reduce-scatter.2.cloned.1.call-start = ((), (), s32[]{:S(2)}) async-start(), calls=%async_computation.5 | async-start | bytes 2621440 | tf_op jit(solution)/shard_map/reduce_scatter | solution.py:104
  12.7 80.5 %copy-start.10 = (f32[512]{0:T(512)S(1)}, f32[512]{0:T(512)}, u32[]{:S(2)}) copy-start(f32[512]{0:T(512)} %param.19) | copy-start | bytes 6148
  12.7 82.3 %copy-start.12 = (f32[2,512]{1,0:T(2,128)S(1)}, f32[2,512]{1,0:T(2,128)}, u32[]{:S(2)}) copy-start(f32[2,512]{1,0:T(2,128)} %param.20) | copy-start | bytes 12292
  90.7 3.8 %collective-permute-start = (bf16[3,512]{1,0:T(4,128)(2,1)S(1)}, bf16[3,512]{1,0:T(4,128)(2,1)S(1)}, u32[]{:S(2)}, u32[]{:S(2)}) collective-permute-start(bf16[3,512]{1,0:T(4,128)(2,1)S(1)} %slice.388), channel_id=1, source_target_pairs={{0,4},{4,8},{8,12},{12,16},{16,20},{20,24},{24,28},{1,5},{5,9},{9,... | collective-permute-start | bytes 9224 | tf_op jit(solution)/shard_map/ppermute | solution.py:13
  95.0 0.8 copy-start.2
  95.1 1.1 copy-start.11
  100.9 26.1 %copy-start.1 = (f32[512,512]{1,0:T(8,128)}, f32[512,512]{1,0:T(8,128)S(1)}, u32[]{:S(2)}) copy-start(f32[512,512]{1,0:T(8,128)S(1)} %convert_multiply_fusion.5) | copy-start | bytes 3145732
  165.9 1.3 copy-start.3
  165.9 1.4 copy-start.4
  175.5 1.1 copy-start.5
  175.5 1.2 copy-start.6
  177.8 2.9 %slice-start = ((f32[512,512]{1,0:T(8,128)}), f32[1,512]{1,0:T(1,128)S(1)}, s32[]{:S(2)}) async-start(f32[512,512]{1,0:T(8,128)} %copy-done.1), calls=%async_computation.6 | async-start | bytes 4096 | tf_op jit(solution)/shard_map/slice | solution.py:97
  177.8 2.9 %copy-start.7 = (f32[255,512]{1,0:T(8,128)S(1)}, f32[255,512]{1,0:T(8,128)}, u32[]{:S(2)}) copy-start(f32[255,512]{1,0:T(8,128)} %get-tuple-element.130) | copy-start | bytes 1566724
  180.8 36.3 %copy-start.8 = (f32[512,512]{1,0:T(8,128)S(1)}, f32[512,512]{1,0:T(8,128)}, u32[]{:S(2)}) copy-start(f32[512,512]{1,0:T(8,128)} %pad.144) | copy-start | bytes 3145732
Sparse Core Ops, SparseCore 0:
  10.7 25.2 all-gather.6
  38.1 49.0 all-gather.8
  89.4 47.6 all-gather.10
  139.0 48.8 all-gather.12
  252.4 28.3 reduce-scatter.1
where the time goes:
time: 288 us; the launch traced here: 287 us
  waiting for transfers between devices  106 us (37%)
  local copies, waits for them, and re-layouts  85.9 us (30%)
  blocking collectives  53.4 us (19%)
  between operations  14.1 us (5%)
  matrix products  13.9 us (5%)
  other arithmetic  10.9 us (4%)
    slice x61, local copies, waits for them, and re-layouts, on_device(): lax.associative_scan(combine_pair, (decay, drive), axis=0)  68.6 us
    all_gather x2, blocking collectives, carried_in(): everything = jax.tree.map(lambda part: lax.all_gather(part, axis), array)  53.4 us
    all_gather x1, waiting for transfers between devices, on_device(): lax.all_gather(proj_x, 'sp', axis=0, tiled=True)  51.2 us
    reduce_scatter x1, waiting for transfers between devices, on_device(): lax.psum_scatter(jnp.dot(mixed, out_cols, preferred_element_type=jnp.floa...  28.5 us
    all_gather x1, waiting for transfers between devices, on_device(): piece = lax.all_gather(normed, 'tp', axis=0, tiled=True)  23.3 us
    pad x32, local copies, waits for them, and re-layouts, on_device(): lax.associative_scan(combine_pair, (decay, drive), axis=0)  11.7 us
    dot_general x1, matrix products, on_device(): jnp.dot(mixed, out_cols, preferred_element_type=jnp.float32)  7.88 us
  transfers between devices with their start and end apart: 6, of which 4 were waited for; matrix products, arithmetic and copies ran while one was open for 34% of the time, Pallas kernels for 0%

commit v1 on v0

--- a/solution.py
+++ b/solution.py
@@ -58,7 +58,12 @@
         lax.all_gather(gate_projection, "sp", axis=0, tiled=True),
     )
     local_width = proj_x.shape[1]
-    piece = lax.all_gather(normed, "tp", axis=0, tiled=True)
+    ring = [normed]
+    for hop in range(3):
+        ring.append(lax.ppermute(ring[-1], "tp", [(dev, (dev + 1) % 4) for dev in range(4)]))
+    piece = jnp.roll(
+        jnp.concatenate(ring[::-1], axis=0), (lax.axis_index("tp") + 1) * ring[0].shape[0], axis=0
+    )
     branch_piece = jnp.dot(piece, full_x, preferred_element_type=jnp.float32).astype(jnp.bfloat16)
     gating_piece = jnp.dot(piece, full_gate, preferred_element_type=jnp.float32).astype(
         jnp.bfloat16

time: 288 us -> 348 us (1.21)
  local copies, waits for them, and re-layouts: 85.9 us -> 150 us
  waiting for transfers between devices: 106 us -> 72.8 us
  other arithmetic: 10.9 us -> 38.1 us
    slice x61 -> x60, local copies, waits for them, and re-layouts: 68.6 us -> 130 us  [on_device(): lax.associative_scan(combine_pair, (decay, drive), axis=0)]
    all_gather x1, waiting for transfers between devices: 51.2 us -> 16.5 us  [on_device(): lax.all_gather(proj_x, 'sp', axis=0, tiled=True)]
    ppermute x0 -> x3, waiting for transfers between devices: none -> 25 us  [on_device(): lax.ppermute(ring[-1], 'tp', [(dev, (dev + 1) % 4) for dev in range(4)])]
    all_gather x1 -> x0, waiting for transfers between devices: 23.3 us -> none  [on_device(): piece = lax.all_gather(normed, 'tp', axis=0, tiled=True)]
    add x16, other arithmetic: 2.9 us -> 17.1 us  [combine_pair(): return (earlier[0] * later[0], later[0] * earlier[1] + later[1])]
    concatenate x15, other arithmetic: 0.28 us -> 7.94 us  [on_device(): lax.associative_scan(combine_pair, (decay, drive), axis=0)]
    unnamed x32 -> x46, local copies, waits for them, and re-layouts: 3.97 us -> 9.2 us
  transfers between devices with their start and end apart: 6 -> 8, of which waited for: 4 -> 6; matrix products, arithmetic and copies ran while one was open for 34% -> 56% of each run, Pallas kernels for 0% -> 0%
where the time goes in v1:
time: 348 us; the launch traced here: 344 us
  local copies, waits for them, and re-layouts  150 us (43%)
  waiting for transfers between devices  72.8 us (21%)
  blocking collectives  53.6 us (15%)
  other arithmetic  38.1 us (11%)
  between operations  13.8 us (4%)
  matrix products  12.5 us (4%)
    slice x60, local copies, waits for them, and re-layouts, on_device(): lax.associative_scan(combine_pair, (decay, drive), axis=0)  130 us
    all_gather x2, blocking collectives, carried_in(): everything = jax.tree.map(lambda part: lax.all_gather(part, axis), array)  53.6 us
    reduce_scatter x1, waiting for transfers between devices, on_device(): lax.psum_scatter(jnp.dot(mixed, out_cols, preferred_element_type=jnp.floa...  28.5 us
    ppermute x3, waiting for transfers between devices, on_device(): lax.ppermute(ring[-1], 'tp', [(dev, (dev + 1) % 4) for dev in range(4)])  25 us
    add x16, other arithmetic, combine_pair(): return (earlier[0] * later[0], later[0] * earlier[1] + later[1])  17.1 us
    all_gather x1, waiting for transfers between devices, on_device(): lax.all_gather(proj_x, 'sp', axis=0, tiled=True)  16.5 us
    pad x32, local copies, waits for them, and re-layouts, on_device(): lax.associative_scan(combine_pair, (decay, drive), axis=0)  10.8 us
    unnamed x46, local copies, waits for them, and re-layouts  9.2 us
  transfers between devices with their start and end apart: 8, of which 6 were waited for; matrix products, arithmetic and copies ran while one was open for 56% of the time, Pallas kernels for 0%

profile of v1, /device:TPU:0, one launch (start us, length us, event | category | flops | bytes accessed | tf_op | source)
XLA Modules:
  0.0 344.5 jit_solution(547599991704164293)
XLA Ops:
  11.8 8.8 %collective-permute-done = bf16[128,2048]{1,0:T(8,128)(2,1)S(1)} collective-permute-done((bf16[128,2048]{1,0:T(8,128)(2,1)S(1)}, bf16[128,2048]{1,0:T(8,128)(2,1)S(1)}, u32[]{:S(2)}, u32[]{:S(2)}) %collective-permute-start) | collective-permute-done | bytes 524320 | tf_op jit(solution)/shard_map/ppermute | solution.py:63
  20.5 8.6 %collective-permute-done.1 = bf16[128,2048]{1,0:T(8,128)(2,1)S(1)} collective-permute-done((bf16[128,2048]{1,0:T(8,128)(2,1)S(1)}, bf16[128,2048]{1,0:T(8,128)(2,1)S(1)}, u32[]{:S(2)}, u32[]{:S(2)}) %collective-permute-start.1) | collective-permute-done | bytes 524320 | tf_op jit(solution)/shard_map/ppermute | solution.py:63
  30.1 7.7 %collective-permute-done.2 = bf16[128,2048]{1,0:T(8,128)(2,1)S(1)} collective-permute-done((bf16[128,2048]{1,0:T(8,128)(2,1)S(1)}, bf16[128,2048]{1,0:T(8,128)(2,1)S(1)}, u32[]{:S(2)}, u32[]{:S(2)}) %collective-permute-start.2) | collective-permute-done | bytes 524320 | tf_op jit(solution)/shard_map/ppermute | solution.py:63
  44.8 16.5 %all-gather.6.cloned.1.call-done = bf16[2048,512]{1,0:T(8,128)(2,1)} async-done(((bf16[256,512]{1,0:T(8,128)(2,1)}), bf16[2048,512]{1,0:T(8,128)(2,1)}) %all-gather.6.cloned.1.call-update) | async-done | bytes 2097168 | tf_op jit(solution)/shard_map/all_gather | solution.py:57
  61.3 3.5 %fusion.15 = bf16[512,512]{1,0:T(8,128)(2,1)S(1)} fusion(bf16[2048,512]{1,0:T(8,128)(2,1)} %all-gather.6.cloned.1.call-done, bf16[1024,2048]{1,0:T(8,128)(2,1)} %constant_dynamic-update-slice_fusion, s32[]{:T(128)S(6)} %select_n.40), kind=kOutput, calls=%fused_computation.27 | convolution fusion | flops 1074003968 | bytes 4718596 | tf_op jit(solution)/shard_map/dot_general | solution.py:67
  64.8 2.6 collective-permute-start.3
  72.4 2.2 slice.304
  74.7 2.1 slice.305
  76.7 19.4 %slice.303 = f32[256,512]{0,1:T(8,128)S(1)} slice(f32[512,512]{0,1:T(8,128)S(1)} %bitcast.47), slice={[1:512:2], [0:512:1]} | slice | bytes 1048576 | tf_op jit(solution)/shard_map/slice | solution.py:102
  96.2 19.5 %slice.307 = f32[256,512]{0,1:T(8,128)S(1)} slice(f32[512,512]{0,1:T(8,128)S(1)} %bitcast.48), slice={[0:511:2], [0:512:1]} | slice | bytes 1048576 | tf_op jit(solution)/shard_map/slice | solution.py:102
  117.7 1.7 multiply_add_fusion
  124.9 2.1 multiply_add_fusion.1
  133.3 1.8 multiply_add_fusion.2
  195.2 2.1 slice.367
  197.3 19.9 %slice.302 = f32[255,512]{0,1:T(8,128)} slice(f32[512,512]{0,1:T(8,128)S(1)} %bitcast.49), slice={[2:512:2], [0:512:1]} | slice | bytes 1044480 | tf_op jit(solution)/shard_map/slice | solution.py:102
  230.8 2.0 copy.35
  232.9 2.5 fusion.43
  236.4 2.1 pad.127
  239.6 2.8 pad.126
  243.1 27.5 %all-gather.1 = f32[8,1,512]{2,1,0:T(1,128)S(1)} all-gather(f32[1,1,512]{2,1,0:T(1,128)S(1)} %add_bitcast_fusion), channel_id=1, replica_groups=mesh['sp'=8,'tp'=4] {'sp'}, dimensions={0}, use_global_device_ids=true | all-gather | bytes 18432 | tf_op jit(solution)/shard_map/all_gather | solution.py:18
  270.6 2.7 pad.145
  275.3 26.1 %all-gather = f32[8,1,512]{2,1,0:T(1,128)S(1)} all-gather(f32[1,1,512]{2,1,0:T(1,128)S(1)} %add_bitcast_fusion.1), channel_id=1, replica_groups=mesh['sp'=8,'tp'=4] {'sp'}, dimensions={0}, use_global_device_ids=true | all-gather | bytes 18432 | tf_op jit(solution)/shard_map/all_gather | solution.py:18
  301.9 7.5 %convolution_convert_fusion = bf16[512,2048]{1,0:T(8,128)(2,1)} fusion(bf16[512,2048]{1,0:T(8,128)(2,1)} %all-gather.10.cloned.1.call-done, bf16[2048,512]{1,0:T(8,128)(2,1)} %all-gather.8.cloned.1.call-done, bf16[1024,2048]{1,0:T(8,128)(2,1)} %constant_dynamic-update-slice_fusion, s32[]{:T(128)S(6)} %select_n.40, f32[512,512]{1,0:T(8,128)S(1)} %pad.144, ...), kind=kOutput, calls=%fused_computation.3 | convolution fusion | flops 2152726528 | bytes 12584964 | tf_op jit(solution)/shard_map/dot_general | solution.py:110
  309.4 28.5 %reduce-scatter.2.cloned.1.call-done = bf16[128,2048]{1,0:T(8,128)(2,1)} async-done(((bf16[512,2048]{1,0:T(8,128)(2,1)}), bf16[128,2048]{1,0:T(8,128)(2,1)}) %reduce-scatter.2.cloned.1.call-update) | async-done | bytes 524304 | tf_op jit(solution)/shard_map/reduce_scatter | solution.py:109
  (220 shorter events, 110.8 us)
Async XLA Ops:
  6.5 62.7 %copy-start = (bf16[2,256,256]{2,1,0:T(8,128)(2,1)S(1)}, bf16[2,256,256]{2,1,0:T(8,128)(2,1)}, u32[]{:S(2)}) copy-start(bf16[2,256,256]{2,1,0:T(8,128)(2,1)} %param.17) | copy-start | bytes 786436
  6.5 33.8 %copy-start.1 = (bf16[128,2048]{1,0:T(8,128)(2,1)S(1)}, bf16[128,2048]{1,0:T(8,128)(2,1)}, u32[]{:S(2)}) copy-start(bf16[128,2048]{1,0:T(8,128)(2,1)} %param.12) | copy-start | bytes 1572868
  6.5 54.8 %all-gather.6.cloned.1.call-start = ((), (), s32[]{:S(2)}) async-start(), calls=%async_computation.1 | async-start | bytes 2359296 | tf_op jit(solution)/shard_map/all_gather | solution.py:57
  7.3 294.6 %all-gather.10.cloned.1.call-start = ((), (), s32[]{:S(2)}) async-start(), calls=%async_computation.3 | async-start | bytes 2359296 | tf_op jit(solution)/shard_map/all_gather | solution.py:108
  8.0 293.9 %all-gather.8.cloned.1.call-start = ((), (), s32[]{:S(2)}) async-start(), calls=%async_computation.2 | async-start | bytes 2359296 | tf_op jit(solution)/shard_map/all_gather | solution.py:58
  11.2 9.3 %collective-permute-start = (bf16[128,2048]{1,0:T(8,128)(2,1)S(1)}, bf16[128,2048]{1,0:T(8,128)(2,1)S(1)}, u32[]{:S(2)}, u32[]{:S(2)}) collective-permute-start(bf16[128,2048]{1,0:T(8,128)(2,1)S(1)} %fusion.23), channel_id=1, source_target_pairs={{0,1},{1,2},{2,3},{3,0},{4,5},{5,6},{6,7},{7,4},{8,9},{9,10},{10,1... | collective-permute-start | bytes 1572872 | tf_op jit(solution)/shard_map/ppermute | solution.py:63
  20.5 8.6 %collective-permute-start.1 = (bf16[128,2048]{1,0:T(8,128)(2,1)S(1)}, bf16[128,2048]{1,0:T(8,128)(2,1)S(1)}, u32[]{:S(2)}, u32[]{:S(2)}) collective-permute-start(bf16[128,2048]{1,0:T(8,128)(2,1)S(1)} %collective-permute-done), channel_id=1, source_target_pairs={{0,1},{1,2},{2,3},{3,0},{4,5},{5,6},{6,7},{7,4},{8,9},{9,10},{10,1... | collective-permute-start | bytes 1572872 | tf_op jit(solution)/shard_map/ppermute | solution.py:63
  29.2 8.6 %collective-permute-start.2 = (bf16[128,2048]{1,0:T(8,128)(2,1)S(1)}, bf16[128,2048]{1,0:T(8,128)(2,1)S(1)}, u32[]{:S(2)}, u32[]{:S(2)}) collective-permute-start(bf16[128,2048]{1,0:T(8,128)(2,1)S(1)} %collective-permute-done.1), channel_id=1, source_target_pairs={{0,1},{1,2},{2,3},{3,0},{4,5},{5,6},{6,7},{7,4},{8,9},{9,10},{10,1... | collective-permute-start | bytes 1572872 | tf_op jit(solution)/shard_map/ppermute | solution.py:63
  29.2 308.8 %reduce-scatter.2.cloned.1.call-start = ((), (), s32[]{:S(2)}) async-start(), calls=%async_computation.4 | async-start | bytes 2621440 | tf_op jit(solution)/shard_map/reduce_scatter | solution.py:109
  43.8 23.6 %copy-start.14 = (f32[512]{0:T(512)S(1)}, f32[512]{0:T(512)}, u32[]{:S(2)}) copy-start(f32[512]{0:T(512)} %param.19) | copy-start | bytes 6148
  44.8 24.4 %copy-start.16 = (f32[2,512]{1,0:T(2,128)S(1)}, f32[2,512]{1,0:T(2,128)}, u32[]{:S(2)}) copy-start(f32[2,512]{1,0:T(2,128)} %param.20) | copy-start | bytes 12292
  64.8 5.1 %copy-start.15 = (bf16[2,256,256]{2,1,0:T(8,128)(2,1)S(1)}, bf16[2,256,256]{2,1,0:T(8,128)(2,1)}, u32[]{:S(2)}) copy-start(bf16[2,256,256]{2,1,0:T(8,128)(2,1)} %param.18) | copy-start | bytes 786436
  64.8 3.9 %collective-permute-start.3 = (bf16[3,512]{1,0:T(4,128)(2,1)S(1)}, bf16[3,512]{1,0:T(4,128)(2,1)S(1)}, u32[]{:S(2)}, u32[]{:S(2)}) collective-permute-start(bf16[3,512]{1,0:T(4,128)(2,1)S(1)} %slice.388), channel_id=1, source_target_pairs={{0,4},{4,8},{8,12},{12,16},{16,20},{20,24},{24,28},{1,5},{5,9},{9,... | collective-permute-start | bytes 9224 | tf_op jit(solution)/shard_map/ppermute | solution.py:13
  69.9 127.5 %copy-start.2 = (f32[512,2,256]{0,2,1:T(8,128)}, f32[512,2,256]{0,2,1:T(8,128)S(1)}, u32[]{:S(2)}) copy-start(f32[512,2,256]{0,2,1:T(8,128)S(1)} %get-tuple-element.172) | copy-start | bytes 3145732
  194.7 32.8 %copy-start.7 = (f32[63,512]{1,0:T(8,128)S(1)}, f32[63,512]{1,0:T(8,128)}, u32[]{:S(2)}) copy-start(f32[63,512]{1,0:T(8,128)} %slice.363) | copy-start | bytes 387076
  195.2 30.8 %copy-start.8 = (f32[31,512]{1,0:T(8,128)S(1)}, f32[31,512]{1,0:T(8,128)}, u32[]{:S(2)}) copy-start(f32[31,512]{1,0:T(8,128)} %slice.320) | copy-start | bytes 190468
  195.2 30.8 %copy-start.9 = (f32[31,512]{1,0:T(8,128)S(1)}, f32[31,512]{1,0:T(8,128)}, u32[]{:S(2)}) copy-start(f32[31,512]{1,0:T(8,128)} %slice.361) | copy-start | bytes 190468
  222.3 5.4 %copy-start.13 = (f32[1,512]{1,0:T(1,128)S(1)}, f32[1,512]{1,0:T(1,128)}, u32[]{:S(2)}) copy-start(f32[1,512]{1,0:T(1,128)} %slice.424) | copy-start | bytes 6148
  223.7 5.6 %copy-start.5 = (f32[127,512]{1,0:T(8,128)S(1)}, f32[127,512]{1,0:T(8,128)}, u32[]{:S(2)}) copy-start(f32[127,512]{1,0:T(8,128)} %slice.308) | copy-start | bytes 780292
  223.7 5.6 %copy-start.6 = (f32[127,512]{1,0:T(8,128)S(1)}, f32[127,512]{1,0:T(8,128)}, u32[]{:S(2)}) copy-start(f32[127,512]{1,0:T(8,128)} %slice.365) | copy-start | bytes 780292
  226.7 2.7 copy-start.12
  227.6 2.0 copy-start.11
  236.3 38.1 %copy-start.4 = (f32[255,512]{1,0:T(8,128)S(1)}, f32[255,512]{1,0:T(8,128)}, u32[]{:S(2)}) copy-start(f32[255,512]{1,0:T(8,128)} %get-tuple-element.131) | copy-start | bytes 1566724
  236.4 65.1 %copy-start.10 = (f32[512]{0:T(512)S(1)}, f32[512]{0:T(512)}, u32[]{:S(2)}) copy-start(f32[512]{0:T(512)} %custom-call) | copy-start | bytes 6148
  (1 other events, 1.6 us)
Sparse Core Ops, SparseCore 0:
  9.5 51.7 all-gather.5
  63.3 48.8 all-gather.9
  114.4 47.3 all-gather.7
  309.5 28.3 reduce-scatter.1
